TPU v7x, 128 devices: a whole 4x4x4 slice. The times are simulated.
128 devices in a mesh: sp: 16 (over z, x), tp: 8 (over y, core).
Axes of the slice: x: 4, y: 4, z: 4, core: 2. Of those that a mesh axis runs over, the one named last changes fastest.
Arguments:
- query_small: bfloat16 [12288, 1024], P('sp', 'tp'), may hold values from -18 to 18
- key_small: bfloat16 [12288, 1024], P('sp', 'tp'), may hold values from -6 to 6
- value_small: bfloat16 [12288, 1024], P('sp', 'tp'), may hold values from -6 to 6
- offset_small: bfloat16 [16, 12288], P('tp', 'sp'), may hold values from -25 to 0
- query_large: bfloat16 [12288, 1024], P('sp', 'tp'), may hold values from -18 to 18
- key_large: bfloat16 [12288, 1024], P('sp', 'tp'), may hold values from -6 to 6
- value_large: bfloat16 [12288, 1024], P('sp', 'tp'), may hold values from -6 to 6
- offset_large: bfloat16 [8, 12288], P('tp', 'sp'), may hold values from -25 to 0
- out_small: bfloat16 [1024, 2048], P('tp'), may hold values from -0.125 to 0.125
- out_large: bfloat16 [1024, 2048], P('tp'), may hold values from -0.125 to 0.125
- residual: bfloat16 [12288, 2048], P(('sp', 'tp')), may hold values from -1.1953125 to 1.1953125
- norm_gain: bfloat16 [2048], replicated, may hold values from 0.099609375 to 1.8984375
- gate_weight: bfloat16 [2048, 5632], P('sp', 'tp'), may hold values from -0.125 to 0.125
- up_weight: bfloat16 [2048, 5632], P('sp', 'tp'), may hold values from -0.125 to 0.125
- down_weight: bfloat16 [5632, 2048], P('tp', 'sp'), may hold values from -0.078125 to 0.078125
Outputs:
- layer_out: bfloat16 [12288, 2048], P(('sp', 'tp'))
All inputs are finite; a program needn't handle non-finite values.
Results may differ from a plain program's by a relative error of at most 0.023.
Values may be sent and summed in bfloat16 or wider, within the bound.
No kernel may reach another device: no remote copies, remote signals or barrier semaphores. Data moves between devices by JAX's collectives and lax.ppermute only.
A program may use at most 128 MiB of HBM per device.

v0:
```python
import jax
import jax.numpy as jnp
from jax import lax
from jax.sharding import PartitionSpec as P

SMALL_DIM = 64
LARGE_DIM = 128


def turned_gather(arrays, axis, dims):
    turned = [jnp.moveaxis(a, dim, 0) for a, dim in zip(arrays, dims)]
    both = jnp.concatenate([t.reshape(len(t), -1) for t in turned], axis=1)
    whole, at, done = (lax.all_gather(both, axis, axis=0, tiled=True), 0, [])
    for t, dim in zip(turned, dims):
        share = whole[:, at : at + t[0].size].reshape(-1, *t.shape[1:])
        done.append(jnp.moveaxis(share, 0, dim))
        at += t[0].size
    return tuple(done)


def cut_along(value, dim, length):
    before, after = (value.shape[:dim], value.shape[dim + 1 :])
    return jnp.moveaxis(value.reshape(*before, length, -1, *after), dim, 0)


def summed_on_arrival(value, axis, dim):
    pieces = cut_along(value, dim, lax.axis_size(axis))
    arrived = lax.all_to_all(pieces, axis, split_axis=0, concat_axis=0, tiled=True)
    return arrived.astype(jnp.float32).sum(axis=0)


def split_heads(flat, head_depth):
    return flat.reshape(flat.shape[0], -1, head_depth)


def stick_terms(query, random_keys, values, offset, limits, carried):
    head_depth = query.shape[-1]
    key_heads = split_heads(random_keys, head_depth)
    value_heads = split_heads(values, head_depth)
    logits = jnp.einsum(
        "thd,shd->hts", query, key_heads, preferred_element_type=jnp.float32
    ) * head_depth ** (-0.5)
    logits = logits + offset.astype(jnp.float32)[:, None, :]
    fail_all = jax.nn.log_sigmoid(-logits)
    log_pass = logits + fail_all
    log_fail = fail_all
    before = None
    if limits is not None:
        query_first, key_first = limits
        query_pos = lax.broadcasted_iota(jnp.int32, logits.shape, 1) + query_first
        key_pos = lax.broadcasted_iota(jnp.int32, logits.shape, 2) + key_first
        before = key_pos < query_pos
        log_fail = jnp.where(before, fail_all, 0.0)
    suffix = lax.cumsum(log_fail, axis=2, reverse=True) - log_fail
    weights = jnp.exp(log_pass + suffix + carried[:, :, None])
    if before is not None:
        weights = jnp.where(before, weights, 0.0)
    weights = weights.astype(jnp.bfloat16)
    result = jnp.einsum("hts,shd->thd", weights, value_heads, preferred_element_type=jnp.float32)
    return (result, carried + jnp.sum(log_fail, axis=2))


def both_groups(queries, key_block, limits, totals):
    key_small, value_small, offset_small, key_large, value_large, offset_large = key_block
    out_small, acc_small, out_large, acc_large = totals
    term_small, next_small = stick_terms(
        queries[0], key_small, value_small, offset_small, limits, acc_small
    )
    term_large, next_large = stick_terms(
        queries[1], key_large, value_large, offset_large, limits, acc_large
    )
    return (out_small + term_small, next_small, out_large + term_large, next_large)


def empty_totals(rows, small_heads, large_heads):
    return (
        jnp.zeros((rows, small_heads, SMALL_DIM), jnp.float32),
        jnp.zeros((small_heads, rows), jnp.float32),
        jnp.zeros((rows, large_heads, LARGE_DIM), jnp.float32),
        jnp.zeros((large_heads, rows), jnp.float32),
    )


def rounded(value):
    return lax.optimization_barrier(value.astype(jnp.bfloat16)).astype(jnp.float32)


def rms_norm(stream, gain):
    scale = lax.rsqrt(jnp.mean(stream * stream, axis=-1, keepdims=True) + 1e-06)
    return (stream * scale * gain.astype(jnp.float32)).astype(jnp.bfloat16)


def on_device(
    query_small,
    key_small,
    value_small,
    offset_small,
    query_large,
    key_large,
    value_large,
    offset_large,
    out_small,
    out_large,
    residual,
    norm_gain,
    gate_weight,
    up_weight,
    down_weight,
):
    gate_full, up_full, down_full = turned_gather(
        (gate_weight, up_weight, down_weight), "sp", (0, 0, 1)
    )
    tokens = query_small.shape[0]
    small_heads = offset_small.shape[0]
    large_heads = offset_large.shape[0]
    queries = (split_heads(query_small, SMALL_DIM), split_heads(query_large, LARGE_DIM))
    own_block = (key_small, value_small, offset_small, key_large, value_large, offset_large)
    sp_index = lax.axis_index("sp")
    own_start = sp_index * tokens
    totals = both_groups(
        queries, own_block, (own_start, own_start), empty_totals(tokens, small_heads, large_heads)
    )
    key_dims = (0, 0, 1, 0, 0, 1)
    gathered = turned_gather(
        (own_block[0], own_block[1], own_block[2], own_block[3], own_block[4], own_block[5]),
        "sp",
        (0, 0, 1, 0, 0, 1),
    )

    def far_turn(turn_index, status):
        first_row = (sp_index - 1 - turn_index) * tokens
        key_block = tuple(
            (
                lax.dynamic_slice_in_dim(member, first_row, tokens, member_dim)
                for member, member_dim in zip(gathered, key_dims)
            )
        )
        return both_groups(queries, key_block, None, status)

    totals = lax.fori_loop(0, sp_index, far_turn, totals)
    mixed_small = totals[0].reshape(tokens, -1).astype(jnp.bfloat16)
    mixed_large = totals[2].reshape(tokens, -1).astype(jnp.bfloat16)
    attended = summed_on_arrival(
        (
            jnp.dot(mixed_small, out_small, preferred_element_type=jnp.float32)
            + jnp.dot(mixed_large, out_large, preferred_element_type=jnp.float32)
        ).astype(jnp.bfloat16),
        "tp",
        0,
    )
    stream = residual.astype(jnp.float32) + rounded(attended)
    normed = rms_norm(stream, norm_gain)
    normed_rows = lax.all_gather(normed, "tp", axis=0, tiled=True)
    gate = jnp.dot(normed_rows, gate_full, preferred_element_type=jnp.float32)
    upper = jnp.dot(normed_rows, up_full, preferred_element_type=jnp.float32)
    hidden = (jax.nn.silu(gate) * upper).astype(jnp.bfloat16)
    summed = lax.psum_scatter(
        jnp.dot(hidden, down_full, preferred_element_type=jnp.float32).astype(jnp.bfloat16),
        "tp",
        scatter_dimension=0,
        tiled=True,
    ).astype(jnp.float32)
    return (stream + rounded(summed)).astype(jnp.bfloat16)


def solution(mesh):
    return jax.shard_map(
        on_device,
        mesh=mesh,
        in_specs=(
            P("sp", "tp"),
            P("sp", "tp"),
            P("sp", "tp"),
            P("tp", "sp"),
            P("sp", "tp"),
            P("sp", "tp"),
            P("sp", "tp"),
            P("tp", "sp"),
            P("tp", None),
            P("tp", None),
            P(("sp", "tp"), None),
            P(),
            P("sp", "tp"),
            P("sp", "tp"),
            P("tp", "sp"),
        ),
        out_specs=P(("sp", "tp"), None),
        check_vma=False,
    )
```

profile of v0, /device:TPU:0, one launch (start us, length us, event | category | flops | bytes accessed | tf_op | source)
XLA Modules:
  0.0 1112.9 jit_solution(5923392795557188407)
XLA Ops:
  6.6 0.0 all-gather.4.cloned.1.call-start
  6.7 1.0 copy.47
  7.6 0.9 copy.48
  8.5 3.2 concatenate.6
  11.7 0.0 all-gather.4.cloned.1.call-update
  11.7 0.0 all-gather.8.cloned.1.call-start
  11.8 0.8 pad_maximum_fusion
  12.7 0.1 copy.40
  12.8 0.8 copy.43
  13.7 3.2 fusion.59
  17.0 7.9 fusion.38
  24.9 2.2 copy.46
  27.1 0.8 copy.39
  28.0 2.4 fusion.54
  30.4 3.9 fusion.60
  34.4 15.1 %fusion.33 = f32[2,768,6,128]{1,2,3,0:T(8,128)S(1)} fusion(f32[2,768,6,128]{1,3,2,0:T(8,128)S(1)} %bitcast.216), kind=kOutput, calls=%fused_computation.58 | output fusion | flops 149815296 | bytes 9437184 | tf_op jit(solution)/shard_map/reduce-window.4
  49.5 2.7 copy-done.4
  52.3 0.1 reduce-window.49
  52.3 4.7 broadcast_add_fusion.1
  57.1 1.4 copy.42
  58.5 0.9 copy-done.3
  59.4 0.1 copy-done.12
  59.5 18.9 %fusion.35 = bf16[2,768,768]{1,2,0:T(8,128)(2,1)S(1)} fusion(f32[2,768,768]{1,2,0:T(8,128)S(1)} %copy-done.3, f32[2,768,6,128]{1,3,2,0:T(8,128)S(1)} %copy.42, f32[2,768,768]{1,2,0:T(8,128)S(1)} %bitcast.219, f32[2,768]{1,0:T(2,128)S(1)} %convert_element_type.74, s32[768]{0:T(1024)S(1)} %iota_add_fusion, u8[768,768]{0,1:T(8,128)(4,1)S(1)} %copy-done.12), kind=kLoop, calls=%fused_computation.63 | loop fusion | flops 21233664 | bytes 17114112 | tf_op jit(solution)/shard_map/convert_element_type | solution.py:58
  78.5 5.6 fusion.45
  84.2 1.1 convolution_bitcast_fusion.3
  85.3 1.3 convolution_bitcast_fusion.2
  86.6 33.8 %all-gather.4.cloned.1.call-done = bf16[12288,515]{1,0:T(8,128)(2,1)} async-done(((bf16[768,515]{1,0:T(8,128)(2,1)}), bf16[12288,515]{1,0:T(8,128)(2,1)}) %all-gather.4.cloned.1.call-update) | async-done | bytes 12656656 | tf_op jit(solution)/shard_map/all_gather | solution.py:13
  120.3 3.2 slice_bitcast_fusion.3
  123.6 3.2 copy.52
  126.8 3.5 slice_reduce_fusion
  130.4 12.6 %fusion.61 = (bf16[12288,128]{1,0:T(8,128)(2,1)}, bf16[12288,128]{1,0:T(8,128)(2,1)}, bf16[12288,128]{1,0:T(8,128)(2,1)}, bf16[12288,128]{1,0:T(8,128)(2,1)}) fusion(bf16[12288,515]{1,0:T(8,128)(2,1)} %all-gather.4.cloned.1.call-done), kind=kLoop, calls=%fused_computation.112 | loop fusion | bytes 25165824 | tf_op jit(solution)/shard_map/slice | solution.py:15
  143.0 1.0 convert_element_type.77
  144.0 1.0 fusion.62
  145.0 0.1 copy-done.17
  145.2 2.7 add_convert_fusion
  147.9 4.6 all-to-all-start
  152.5 0.0 all-gather.6.cloned.1.call-start
  152.5 38.3 %all-to-all-done = bf16[8,96,2048]{2,1,0:T(8,128)(2,1)} async-done(((bf16[8,96,2048]{2,1,0:T(8,128)(2,1)}), bf16[8,96,2048]{2,1,0:T(8,128)(2,1)}, u32[]{:S(2)}, u32[]{:S(2)}) %all-to-all-start) | async-done | bytes 3145760 | tf_op jit(solution)/shard_map/all_to_all | solution.py:28
  190.9 2.6 reduce_sum.64
  193.5 0.2 multiply_reduce_fusion
  193.7 0.9 multiply_convert_fusion.1
  194.7 0.0 reduce-scatter.2.cloned.1.call-start
  194.7 6.0 all-gather.8.cloned.1.call-done
  200.7 850.4 %all-gather.6.cloned.1.call-done = bf16[768,2048]{1,0:T(8,128)(2,1)} async-done(((bf16[96,2048]{1,0:T(8,128)(2,1)}), bf16[768,2048]{1,0:T(8,128)(2,1)}) %all-gather.6.cloned.1.call-update) | async-done | bytes 3145744 | tf_op jit(solution)/shard_map/all_gather | solution.py:153
  1051.1 5.2 fusion.43
  1056.3 11.8 %convolution_convert_fusion = bf16[768,2048]{1,0:T(8,128)(2,1)} fusion(bf16[2048,2112]{0,1:T(8,128)(2,1)} %all-gather.8.cloned.1.call-done, f32[768,704]{0,1:T(8,128)S(1)} %fusion.43, bf16[768,2048]{1,0:T(8,128)(2,1)} %all-gather.6.cloned.1.call-done), kind=kOutput, calls=%fused_computation.71 | convolution fusion | flops 4434001920 | bytes 14221312 | tf_op jit(solution)/shard_map/dot_general | solution.py:158
  1068.2 36.1 %reduce-scatter.2.cloned.1.call-done = bf16[96,2048]{1,0:T(8,128)(2,1)} async-done(((bf16[768,2048]{1,0:T(8,128)(2,1)}), bf16[96,2048]{1,0:T(8,128)(2,1)}) %reduce-scatter.2.cloned.1.call-update) | async-done | bytes 393232 | tf_op jit(solution)/shard_map/reduce_scatter | solution.py:157
  1104.2 1.9 add_convert_fusion.1
  (65 shorter events, 0.3 us)
Async XLA Ops:
  6.5 137.5 %copy-start = (bf16[128,2048]{1,0:T(8,128)(2,1)S(1)}, bf16[128,2048]{1,0:T(8,128)(2,1)}, u32[]{:S(2)}) copy-start(bf16[128,2048]{1,0:T(8,128)(2,1)} %param.25) | copy-start | bytes 1572868
  6.5 6.1 copy-start.24
  6.5 7.1 copy-start.23
  6.5 6.1 copy-start.14
  6.5 6.3 copy-start.15
  6.6 7.2 copy-start.18
  6.6 5.2 copy-start.20
  6.6 5.2 copy-start.22
  6.6 5.2 copy-start.21
  6.6 7.1 copy-start.26
  6.6 113.7 %all-gather.4.cloned.1.call-start = ((), (), s32[]{:S(2)}) async-start(), calls=%async_computation.2 | async-start | bytes 16711680 | tf_op jit(solution)/shard_map/all_gather | solution.py:13
  11.7 189.0 %all-gather.8.cloned.1.call-start = ((), (), s32[]{:S(2)}) async-start(), calls=%async_computation.4 | async-start | bytes 9191424 | tf_op jit(solution)/shard_map/all_gather | solution.py:13
  17.0 10.2 copy-start.9
  24.9 2.2 copy-start.19
  30.4 4.0 copy-start.8
  30.4 4.0 copy-start.11
  34.3 15.2 %copy-start.2 = (f32[2,768,768]{1,2,0:T(8,128)}, f32[2,768,768]{1,2,0:T(8,128)S(1)}, u32[]{:S(2)}) copy-start(f32[2,768,768]{1,2,0:T(8,128)S(1)} %get-tuple-element.239) | copy-start | bytes 14155780
  34.4 24.1 %slice-start.2 = ((s8[4718592]{0:T(1024)(128)(4,1)}), s8[524288]{0:T(1024)(128)(4,1)S(1)}, s32[]{:S(2)}) async-start(s8[4718592]{0:T(1024)(128)(4,1)} %bitcast.218), calls=%async_computation.8 | async-start | bytes 1048576
  49.5 2.7 copy-start.4
  52.3 6.1 slice-start.3
  57.0 2.3 copy-start.3
  57.0 2.5 copy-start.12
  78.5 5.6 copy-start.13
  78.5 6.7 copy-start.16
  144.0 1.0 copy-start.7
  144.0 1.2 copy-start.17
  147.9 4.6 copy-start.25
  147.9 43.0 %all-to-all-start = ((bf16[8,96,2048]{2,1,0:T(8,128)(2,1)}), bf16[8,96,2048]{2,1,0:T(8,128)(2,1)}, u32[]{:S(2)}, u32[]{:S(2)}) async-start(bf16[8,96,2048]{2,1,0:T(8,128)(2,1)} %bitcast.220), calls=%async_computation | async-start | bytes 6291456 | tf_op jit(solution)/shard_map/all_to_all | solution.py:28
  152.5 41.0 %copy-start.10 = (bf16[96,2048]{1,0:T(8,128)(2,1)S(1)}, bf16[96,2048]{1,0:T(8,128)(2,1)}, u32[]{:S(2)}) copy-start(bf16[96,2048]{1,0:T(8,128)(2,1)} %param.27) | copy-start | bytes 1179652
  152.5 898.7 %all-gather.6.cloned.1.call-start = ((), (), s32[]{:S(2)}) async-start(), calls=%async_computation.3 | async-start | bytes 3538944 | tf_op jit(solution)/shard_map/all_gather | solution.py:153
  194.7 909.6 %reduce-scatter.2.cloned.1.call-start = ((), (), s32[]{:S(2)}) async-start(), calls=%async_computation.5 | async-start | bytes 3538944 | tf_op jit(solution)/shard_map/reduce_scatter | solution.py:157
Sparse Core Ops, SparseCore 0:
  11.8 108.4 all-gather.3
  122.4 78.2 all-gather.7
  202.4 848.6 all-gather.5
  1068.3 35.9 reduce-scatter.1
where the time goes:
time: 1120 us; the launch traced here: 1110 us
  waiting for transfers between devices  965 us (86%)
  other arithmetic  63.8 us (6%)
  local copies, waits for them, and re-layouts  37.1 us (3%)
  matrix products  28.8 us (3%)
  between operations  13.8 us (1%)
    all_gather x1, waiting for transfers between devices, on_device(): normed_rows = lax.all_gather(normed, 'tp', axis=0, tiled=True)  850 us
    all_gather x2, waiting for transfers between devices, turned_gather(): whole, at, done = (lax.all_gather(both, axis, axis=0, tiled=True), 0, [])  39.8 us
    all_to_all x1, waiting for transfers between devices, summed_on_arrival(): lax.all_to_all(pieces, axis, split_axis=0, concat_axis=0, tiled=True)  38.3 us
    reduce_scatter x1, waiting for transfers between devices, on_device(): lax.psum_scatter(jnp.dot(hidden, down_full, preferred_element_type=jnp.fl...  36.1 us
    convert_element_type x2, other arithmetic, stick_terms(): weights = weights.astype(jnp.bfloat16)  24.5 us
    another operation x4, other arithmetic  23.2 us
  transfers between devices with their start and end apart: 5, of which 5 were waited for; matrix products, arithmetic and copies ran while one was open for 9% of the time, Pallas kernels for 0%

commit v1 on v0

--- a/solution.py
+++ b/solution.py
@@ -5,6 +5,27 @@
 
 SMALL_DIM = 64
 LARGE_DIM = 128
+
+
+def gather_around(x, axis, dim):
+    length, place, rows = (lax.axis_size(axis), lax.axis_index(axis), x.shape[dim])
+    upward = [(i, (i + 1) % length) for i in range(length)]
+    left = [(i, (i - 1) % length) for i in range(length)]
+    out = jnp.zeros((*x.shape[:dim], length * rows, *x.shape[dim + 1 :]), x.dtype)
+    out = lax.dynamic_update_slice_in_dim(out, x, place * rows, axis=dim)
+    from_left = from_right = x
+    half = length // 2
+    for step in range(1, half + 1):
+        from_left = lax.ppermute(from_left, axis, upward)
+        out = lax.dynamic_update_slice_in_dim(
+            out, from_left, (place - step) % length * rows, axis=dim
+        )
+        if step < length - half:
+            from_right = lax.ppermute(from_right, axis, left)
+            out = lax.dynamic_update_slice_in_dim(
+                out, from_right, (place + step) % length * rows, axis=dim
+            )
+    return out
 
 
 def turned_gather(arrays, axis, dims):
@@ -150,7 +171,7 @@
     )
     stream = residual.astype(jnp.float32) + rounded(attended)
     normed = rms_norm(stream, norm_gain)
-    normed_rows = lax.all_gather(normed, "tp", axis=0, tiled=True)
+    normed_rows = gather_around(normed, "tp", 0)
     gate = jnp.dot(normed_rows, gate_full, preferred_element_type=jnp.float32)
     upper = jnp.dot(normed_rows, up_full, preferred_element_type=jnp.float32)
     hidden = (jax.nn.silu(gate) * upper).astype(jnp.bfloat16)

time: 1120 us -> 1130 us (level)
    all_gather x1 -> x0, waiting for transfers between devices: 850 us -> none  [on_device(): normed_rows = lax.all_gather(normed, 'tp', axis=0, tiled=True)]
    reduce_scatter x1, waiting for transfers between devices: 36.1 us -> 864 us  [on_device(): lax.psum_scatter(jnp.dot(hidden, down_full, preferred_element_type=jnp.fl...]
    ppermute x0 -> x7, waiting for transfers between devices: none -> 20.1 us  [the longest x4 20.1 us: gather_around(): from_left = lax.ppermute(from_left, axis, upward)]
  transfers between devices with their start and end apart: 5 -> 11, of which waited for: 5 -> 7; matrix products, arithmetic and copies ran while one was open for 9% -> 10% of each run, Pallas kernels for 0% -> 0%
where the time goes in v1:
time: 1130 us; the launch traced here: 1120 us
  waiting for transfers between devices  956 us (85%)
  other arithmetic  63.9 us (6%)
  local copies, waits for them, and re-layouts  44.7 us (4%)
  matrix products  28.7 us (3%)
  between operations  13.8 us (1%)
  starting transfers between devices  13.6 us (1%)
    reduce_scatter x1, waiting for transfers between devices, on_device(): lax.psum_scatter(jnp.dot(hidden, down_full, preferred_element_type=jnp.fl...  864 us
    all_to_all x1, waiting for transfers between devices, summed_on_arrival(): lax.all_to_all(pieces, axis, split_axis=0, concat_axis=0, tiled=True)  38.3 us
    all_gather x2, waiting for transfers between devices, turned_gather(): whole, at, done = (lax.all_gather(both, axis, axis=0, tiled=True), 0, [])  33.8 us
    convert_element_type x2, other arithmetic, stick_terms(): weights = weights.astype(jnp.bfloat16)  24.5 us
    another operation x4, other arithmetic  23.2 us
  transfers between devices with their start and end apart: 11, of which 7 were waited for; matrix products, arithmetic and copies ran while one was open for 10% of the time, Pallas kernels for 0%

profile of v1, /device:TPU:0, one launch (start us, length us, event | category | flops | bytes accessed | tf_op | source)
XLA Modules:
  0.0 1121.0 jit_solution(922381284366145240)
XLA Ops:
  6.7 1.0 copy.47
  7.6 0.9 copy.48
  8.5 3.2 concatenate.6
  11.8 0.9 pad_maximum_fusion
  12.9 0.8 copy.43
  13.7 3.3 fusion.59
  17.0 7.9 fusion.38
  24.9 2.2 copy.46
  27.1 0.8 copy.39
  28.0 2.4 fusion.50
  30.4 3.9 fusion.60
  34.4 15.1 %fusion.33 = f32[2,768,6,128]{1,2,3,0:T(8,128)S(1)} fusion(f32[2,768,6,128]{1,3,2,0:T(8,128)S(1)} %bitcast.216), kind=kOutput, calls=%fused_computation.58 | output fusion | flops 149815296 | bytes 9437184 | tf_op jit(solution)/shard_map/reduce-window.4
  49.5 2.7 copy-done.4
  52.4 4.7 broadcast_add_fusion.1
  57.1 1.4 copy.42
  58.5 0.9 copy-done.3
  59.5 18.9 %fusion.35 = bf16[2,768,768]{1,2,0:T(8,128)(2,1)S(1)} fusion(f32[2,768,768]{1,2,0:T(8,128)S(1)} %copy-done.3, f32[2,768,6,128]{1,3,2,0:T(8,128)S(1)} %copy.42, f32[2,768,768]{1,2,0:T(8,128)S(1)} %bitcast.219, f32[2,768]{1,0:T(2,128)S(1)} %convert_element_type.74, s32[768]{0:T(1024)S(1)} %iota_add_fusion, u8[768,768]{0,1:T(8,128)(4,1)S(1)} %copy-done.12), kind=kLoop, calls=%fused_computation.63 | loop fusion | flops 21233664 | bytes 17114112 | tf_op jit(solution)/shard_map/convert_element_type | solution.py:79
  78.5 5.6 fusion.45
  84.2 1.1 convolution_bitcast_fusion.3
  85.3 1.3 convolution_bitcast_fusion.2
  86.6 33.7 %all-gather.3.cloned.1.call-done = bf16[12288,515]{1,0:T(8,128)(2,1)} async-done(((bf16[768,515]{1,0:T(8,128)(2,1)}), bf16[12288,515]{1,0:T(8,128)(2,1)}) %all-gather.3.cloned.1.call-update) | async-done | bytes 12656656 | tf_op jit(solution)/shard_map/all_gather | solution.py:34
  120.3 3.2 slice_bitcast_fusion.3
  123.6 3.2 copy.52
  126.8 3.6 slice_reduce_fusion
  130.4 12.6 %fusion.61 = (bf16[12288,128]{1,0:T(8,128)(2,1)}, bf16[12288,128]{1,0:T(8,128)(2,1)}, bf16[12288,128]{1,0:T(8,128)(2,1)}, bf16[12288,128]{1,0:T(8,128)(2,1)}) fusion(bf16[12288,515]{1,0:T(8,128)(2,1)} %all-gather.3.cloned.1.call-done), kind=kLoop, calls=%fused_computation.120 | loop fusion | bytes 25165824 | tf_op jit(solution)/shard_map/slice | solution.py:36
  143.0 1.0 convert_element_type.77
  144.0 1.0 fusion.62
  145.2 2.7 add_convert_fusion
  147.9 4.6 all-to-all-start
  152.5 38.3 %all-to-all-done = bf16[8,96,2048]{2,1,0:T(8,128)(2,1)} async-done(((bf16[8,96,2048]{2,1,0:T(8,128)(2,1)}), bf16[8,96,2048]{2,1,0:T(8,128)(2,1)}, u32[]{:S(2)}, u32[]{:S(2)}) %all-to-all-start) | async-done | bytes 3145760 | tf_op jit(solution)/shard_map/all_to_all | solution.py:49
  190.9 2.6 reduce_sum.64
  193.7 2.1 broadcast_in_dim.8
  195.8 0.9 constant_dynamic-update-slice_fusion.7
  196.7 3.0 collective-permute-start.1
  199.7 5.5 collective-permute-done
  205.1 3.0 collective-permute-start.3
  209.6 3.9 collective-permute-done.2
  213.6 3.0 collective-permute-start.5
  216.5 0.8 constant_dynamic-update-slice_fusion.4
  218.1 3.9 collective-permute-done.4
  222.0 0.8 constant_dynamic-update-slice_fusion.2
  222.8 0.8 constant_dynamic-update-slice_fusion.1
  223.6 6.8 collective-permute-done.6
  230.4 0.8 constant_dynamic-update-slice_fusion
  231.2 5.2 fusion.41
  236.4 11.8 %convolution_convert_fusion = bf16[768,2048]{1,0:T(8,128)(2,1)} fusion(bf16[2048,2112]{0,1:T(8,128)(2,1)} %all-gather.5.cloned.1.call-done, f32[768,704]{0,1:T(8,128)S(1)} %fusion.41, bf16[768,2048]{1,0:T(8,128)(2,1)} %constant_dynamic-update-slice_fusion), kind=kOutput, calls=%fused_computation.71 | convolution fusion | flops 4434001920 | bytes 14221312 | tf_op jit(solution)/shard_map/dot_general | solution.py:179
  248.2 864.2 %reduce-scatter.2.cloned.1.call-done = bf16[96,2048]{1,0:T(8,128)(2,1)} async-done(((bf16[768,2048]{1,0:T(8,128)(2,1)}), bf16[96,2048]{1,0:T(8,128)(2,1)}) %reduce-scatter.2.cloned.1.call-update) | async-done | bytes 393232 | tf_op jit(solution)/shard_map/reduce_scatter | solution.py:178
  1112.4 1.9 add_convert_fusion.1
  (84 shorter events, 3.5 us)
Async XLA Ops:
  6.5 137.5 %copy-start = (bf16[128,2048]{1,0:T(8,128)(2,1)S(1)}, bf16[128,2048]{1,0:T(8,128)(2,1)}, u32[]{:S(2)}) copy-start(bf16[128,2048]{1,0:T(8,128)(2,1)} %param.25) | copy-start | bytes 1572868
  6.5 6.1 copy-start.24
  6.5 7.1 copy-start.23
  6.5 6.1 copy-start.14
  6.5 6.3 copy-start.15
  6.6 7.2 copy-start.18
  6.6 5.2 copy-start.20
  6.6 5.2 copy-start.22
  6.6 5.2 copy-start.21
  6.6 7.1 copy-start.26
  6.6 113.7 %all-gather.3.cloned.1.call-start = ((), (), s32[]{:S(2)}) async-start(), calls=%async_computation.2 | async-start | bytes 16711680 | tf_op jit(solution)/shard_map/all_gather | solution.py:34
  11.7 219.5 %all-gather.5.cloned.1.call-start = ((), (), s32[]{:S(2)}) async-start(), calls=%async_computation.3 | async-start | bytes 9191424 | tf_op jit(solution)/shard_map/all_gather | solution.py:34
  17.0 10.1 copy-start.9
  24.9 2.2 copy-start.19
  30.4 4.0 copy-start.8
  30.4 4.0 copy-start.11
  34.4 15.2 %copy-start.2 = (f32[2,768,768]{1,2,0:T(8,128)}, f32[2,768,768]{1,2,0:T(8,128)S(1)}, u32[]{:S(2)}) copy-start(f32[2,768,768]{1,2,0:T(8,128)S(1)} %get-tuple-element.241) | copy-start | bytes 14155780
  34.4 24.1 %slice-start.2 = ((s8[4718592]{0:T(1024)(128)(4,1)}), s8[524288]{0:T(1024)(128)(4,1)S(1)}, s32[]{:S(2)}) async-start(s8[4718592]{0:T(1024)(128)(4,1)} %bitcast.218), calls=%async_computation.7 | async-start | bytes 1048576
  49.5 2.7 copy-start.4
  52.3 6.1 slice-start.3
  57.0 2.3 copy-start.3
  57.0 2.5 copy-start.12
  78.5 5.6 copy-start.13
  78.5 6.8 copy-start.16
  144.0 1.0 copy-start.7
  144.0 1.2 copy-start.17
  147.9 4.7 copy-start.25
  147.9 43.0 %all-to-all-start = ((bf16[8,96,2048]{2,1,0:T(8,128)(2,1)}), bf16[8,96,2048]{2,1,0:T(8,128)(2,1)}, u32[]{:S(2)}, u32[]{:S(2)}) async-start(bf16[8,96,2048]{2,1,0:T(8,128)(2,1)} %bitcast.220), calls=%async_computation | async-start | bytes 6291456 | tf_op jit(solution)/shard_map/all_to_all | solution.py:49
  152.5 41.0 %copy-start.10 = (bf16[96,2048]{1,0:T(8,128)(2,1)S(1)}, bf16[96,2048]{1,0:T(8,128)(2,1)}, u32[]{:S(2)}) copy-start(bf16[96,2048]{1,0:T(8,128)(2,1)} %param.27) | copy-start | bytes 1179652
  152.5 959.9 %reduce-scatter.2.cloned.1.call-start = ((), (), s32[]{:S(2)}) async-start(), calls=%async_computation.4 | async-start | bytes 3538944 | tf_op jit(solution)/shard_map/reduce_scatter | solution.py:178
  196.7 8.4 collective-permute-start
  196.7 8.4 collective-permute-start.1
  205.1 8.4 collective-permute-start.2
  205.1 8.4 collective-permute-start.3
  213.6 8.4 collective-permute-start.4
  213.6 9.2 collective-permute-start.5
  222.0 8.4 collective-permute-start.6
Sparse Core Ops, SparseCore 0:
  11.8 108.4 all-gather.2
  122.4 78.2 all-gather.4
  248.3 864.0 reduce-scatter.1
